TPU v7x, 256 devices: a whole 4x4x8 slice. The times are simulated.
256 devices in a mesh: sp: 32 (over z, y), tp: 8 (over x, core).
Axes of the slice: x: 4, y: 4, z: 8, core: 2. Of those that a mesh axis runs over, the one named last changes fastest.
Arguments:
- tokens: bfloat16 [32768, 2048], P('sp'), may hold values from -6 to 6
- in_gain: float32 [2048], replicated, may hold values from 0.1 to 1.9
- w_query: bfloat16 [2048, 1024], P(None, 'tp'), may hold values from -0.125 to 0.125
- w_forget: bfloat16 [2048, 1024], P(None, 'tp'), may hold values from -0.125 to 0.125
- w_input: bfloat16 [2048, 1024], P(None, 'tp'), may hold values from -0.125 to 0.125
- w_outgate: bfloat16 [2048, 1024], P(None, 'tp'), may hold values from -0.125 to 0.125
- w_conv_h: bfloat16 [2048, 1024], P(None, 'tp'), may hold values from -0.125 to 0.125
- w_conv_b: bfloat16 [2048, 1024], P(None, 'tp'), may hold values from -0.125 to 0.125
- w_conv_c: bfloat16 [2048, 1024], P(None, 'tp'), may hold values from -0.125 to 0.125
- forget_floor: float32 [1024], P('tp'), may hold values from 0.84 to 1
- forget_leak: float32 [32768, 1024], P('sp', 'tp'), may hold values from -1 to 0
- state_gain: float32 [128], replicated, may hold values from 0.1 to 1.9
- conv_taps: bfloat16 [3, 1024], P(None, 'tp'), may hold values from -3.5 to 3.5
- group_gain: float32 [128], replicated, may hold values from 0.1 to 1.9
- out_state: bfloat16 [1024, 2048], P('tp'), may hold values from -0.1875 to 0.1875
- out_conv: bfloat16 [1024, 2048], P('tp'), may hold values from -0.1875 to 0.1875
Outputs:
- mixed_out: bfloat16 [32768, 2048], P('sp', 'tp')
All inputs are finite; a program needn't handle non-finite values.
Results may differ from a plain program's by a relative error of at most 0.015.
Values may be sent and summed in bfloat16 or wider, within the bound.
No kernel may reach another device: no remote copies, remote signals or barrier semaphores. Data moves between devices by JAX's collectives and lax.ppermute only.
A program may use at most 128 MiB of HBM per device.

v0:
```python
import jax
import jax.numpy as jnp
from jax import lax
from jax.sharding import Mesh
from jax.sharding import PartitionSpec as P

GROUP_FEATURES = 128
BLOCK = 64
TAPS = 3
SP = ("sp_0", "sp_1")
norm_eps = 1e-06


def from_behind(array, axis, by):
    count = lax.axis_size(axis)
    pairs = [(i, i + by) for i in range(count) if 0 <= i + by < count]
    return lax.ppermute(array, axis, pairs)


def neutral_like(array, identity):
    return jax.tree.map(
        lambda part, zero: jnp.zeros_like(part) + jnp.asarray(zero, part.dtype), array, identity
    )


def collected_together(array, axis):
    leaves = jax.tree.leaves(array)
    turns = sorted(range(len(leaves)), key=lambda k: -leaves[k].size)
    width = (1, *leaves[turns[0]].shape)[-1]
    lines = [
        jnp.pad(leaves[k].reshape(-1), (0, -leaves[k].size % width)).reshape(-1, width)
        for k in turns
    ]
    both, at, found = (lax.all_gather(jnp.concatenate(lines), axis), 0, {})
    for k, line in zip(turns, lines):
        section = both[:, at : at + len(line)].reshape(len(both), -1)
        found[k] = section[:, : leaves[k].size].reshape(-1, *leaves[k].shape)
        at += len(line)
    numbers = iter(range(len(leaves)))
    return jax.tree.map(lambda _: found[next(numbers)], array)


def carried_in(array, axes, combine, identity):
    before = start = neutral_like(array, identity)
    subtotal = array
    for axis in reversed(axes):
        count, index = (lax.axis_size(axis), lax.axis_index(axis))
        pieces = collected_together(
            jax.tree.map(
                lambda part, kind: part.astype(kind), subtotal, (jnp.bfloat16, jnp.bfloat16)
            ),
            axis,
        )
        inside, subtotal = (start, start)
        for k in range(count):
            passed = k < index
            subtotal = combine(
                subtotal, jax.tree.map(lambda part, own: part[k].astype(own.dtype), pieces, array)
            )
            inside = jax.tree.map(lambda new, old: jnp.where(passed, new, old), subtotal, inside)
        before = combine(inside, before)
    return before


def rms_rows(values, gain):
    scale = lax.rsqrt(jnp.mean(values * values, axis=-1, keepdims=True) + norm_eps)
    return values * scale * gain


def state_block(carry, inputs):
    carry_state, offset = carry
    query_blk, key_blk, value_blk, logf_blk = inputs
    cum_log = jnp.cumsum(logf_blk, axis=1)
    carried = jnp.einsum("hcd,hde->hce", query_blk * jnp.exp(cum_log), carry_state)
    length = logf_blk.shape[1]
    causal = (jnp.arange(length)[:, None] >= jnp.arange(length)[None, :])[None, :, :, None]
    diff_log = cum_log[:, :, None, :] - cum_log[:, None, :, :]
    decay_all = jnp.exp(jnp.where(causal, diff_log, -jnp.inf))
    scores = jnp.einsum("hid,hjd,hijd->hij", query_blk, key_blk, decay_all)
    result = carried + jnp.einsum("hij,hje->hie", scores, value_blk)
    last_log = cum_log[:, -1, :]
    fresh = jnp.einsum("hcd,hce->hde", key_blk * jnp.exp(last_log[:, None, :] - cum_log), value_blk)
    new_state = jnp.exp(last_log)[:, :, None] * carry_state + fresh
    return ((new_state, offset + last_log), (result, offset[:, None, :] + cum_log))


def join_states(earlier, later):
    earlier_log, earlier_state = earlier
    later_log, later_state = later
    return (earlier_log + later_log, jnp.exp(later_log)[:, :, None] * earlier_state + later_state)


def body(
    tokens,
    in_gain,
    w_query,
    w_forget,
    w_input,
    w_outgate,
    w_conv_h,
    w_conv_b,
    w_conv_c,
    forget_floor,
    forget_leak,
    state_gain,
    conv_taps,
    group_gain,
    out_state,
    out_conv,
):
    count = tokens.shape[0]
    heads = w_query.shape[1] // GROUP_FEATURES
    channels = w_conv_h.shape[1]
    normed = rms_rows(tokens.astype(jnp.float32), in_gain).astype(jnp.bfloat16)

    def project(weight):
        return jnp.dot(normed, weight, preferred_element_type=jnp.float32).astype(jnp.bfloat16)

    proj_query = project(w_query)
    proj_forget = project(w_forget)
    proj_input = project(w_input)
    proj_outgate = project(w_outgate)
    proj_h = project(w_conv_h)
    proj_b = project(w_conv_b)
    proj_c = project(w_conv_c)
    conv_in = (proj_c.astype(jnp.float32) * proj_h.astype(jnp.float32)).astype(jnp.bfloat16)
    rim_rows = from_behind(conv_in[count - (TAPS - 1) :], SP, 1)
    gate_logit = proj_forget.astype(jnp.float32)
    log_forget = (
        jnp.logaddexp(
            jnp.log(forget_floor), jnp.log1p(-forget_floor) + jax.nn.log_sigmoid(gate_logit)
        )
        + forget_leak
    )
    key_gate = (1.0 - forget_floor) * jax.nn.sigmoid(-gate_logit)
    query_act = jax.nn.silu(proj_query.astype(jnp.float32))
    value_f = proj_input.astype(jnp.float32)
    nblk = count // BLOCK

    def to_blocks(arr):
        return arr.reshape(nblk, BLOCK, heads, GROUP_FEATURES).transpose(0, 2, 1, 3)

    def from_blocks(arr):
        return arr.transpose(0, 2, 1, 3).reshape(count, heads, GROUP_FEATURES)

    start_state = jnp.zeros((heads, GROUP_FEATURES, GROUP_FEATURES), jnp.float32)
    start_log = jnp.zeros((heads, GROUP_FEATURES), jnp.float32)
    (local_state, total_log), (local_read, cum_blocks) = lax.scan(
        state_block,
        (start_state, start_log),
        (to_blocks(query_act), to_blocks(key_gate), to_blocks(value_f), to_blocks(log_forget)),
    )
    _, incoming = carried_in((total_log, local_state), SP, join_states, (start_log, start_state))
    cum_device = from_blocks(cum_blocks)
    query_heads = query_act.reshape(count, heads, GROUP_FEATURES)
    cross = jnp.einsum("thd,hde->the", query_heads * jnp.exp(cum_device), incoming)
    state_read = from_blocks(local_read) + cross
    out_gate = jax.nn.silu(proj_outgate.astype(jnp.float32)).reshape(count, heads, GROUP_FEATURES)
    state_res = (
        (rms_rows(state_read, state_gain) * out_gate)
        .reshape(count, heads * GROUP_FEATURES)
        .astype(jnp.bfloat16)
    )
    padded = jnp.concatenate([rim_rows, conv_in], axis=0).astype(jnp.float32)
    taps_f = conv_taps.astype(jnp.float32)
    conv_sum = jnp.zeros((count, channels), jnp.float32)
    for offset in range(TAPS):
        conv_sum = conv_sum + taps_f[offset][None, :] * padded[offset : offset + count]
    gated = (proj_b.astype(jnp.float32) * conv_sum).reshape(
        count, channels // GROUP_FEATURES, GROUP_FEATURES
    )
    conv_res = rms_rows(gated, group_gain).reshape(count, channels).astype(jnp.bfloat16)
    mixed_here = jnp.concatenate([state_res, conv_res], axis=1)
    weight_rows = jnp.concatenate([out_state, out_conv], axis=0)
    columns = lax.all_to_all(weight_rows, "tp", split_axis=1, concat_axis=0, tiled=True)
    summed = jnp.dot(
        lax.all_gather(mixed_here, "tp", axis=1, tiled=True),
        columns,
        preferred_element_type=jnp.float32,
    )
    return summed.astype(jnp.bfloat16)


def solution(mesh):
    split = Mesh(mesh.devices.reshape(8, 4, mesh.shape["tp"]), ("sp_0", "sp_1", "tp"))
    placed = (
        P(SP, None),
        P(),
        P(None, "tp"),
        P(None, "tp"),
        P(None, "tp"),
        P(None, "tp"),
        P(None, "tp"),
        P(None, "tp"),
        P(None, "tp"),
        P("tp"),
        P(SP, "tp"),
        P(),
        P(None, "tp"),
        P(),
        P("tp", None),
        P("tp", None),
    )
    return jax.shard_map(body, mesh=split, in_specs=placed, out_specs=P(SP, "tp"), check_vma=False)
```

profile of v0, /device:TPU:1, one launch (start us, length us, event | category | flops | bytes accessed | tf_op | source)
XLA Modules:
  0.0 187.0 jit_solution(12285283551542501446)
XLA Ops:
  6.5 3.2 %fusion.30 = f32[1024]{0:T(1024)S(1)} fusion(bf16[1024,2048]{1,0:T(8,128)(2,1)} %param.18), kind=kLoop, calls=%fused_computation.44 | loop fusion | flops 6290432 | bytes 4198400 | tf_op jit(solution)/shard_map/reduce_sum | solution.py:66
  10.1 1.0 fusion.32
  11.1 1.2 fusion.37
  12.5 1.3 fusion.36
  13.8 4.0 %collective-permute-start = (bf16[2,128]{1,0:T(2,128)(2,1)S(1)}, bf16[2,128]{1,0:T(2,128)(2,1)S(1)}, u32[]{:S(2)}, u32[]{:S(2)}) collective-permute-start(bf16[2,128]{1,0:T(2,128)(2,1)S(1)} %slice.193), channel_id=1, source_target_pairs={{0,8},{8,16},{16,24},{24,32},{32,40},{40,48},{48,56},{56,64},{64,7... | collective-permute-start | bytes 1544 | tf_op jit(solution)/shard_map/ppermute | solution.py:17
  18.0 3.6 %divide_multiply_fusion = f32[1024,128]{1,0:T(8,128)S(1)} fusion(bf16[1024,2048]{1,0:T(8,128)(2,1)} %copy-done.1, bf16[2048,128]{1,0:T(8,128)(2,1)S(1)} %copy-done.13), kind=kOutput, calls=%fused_computation.83 | convolution fusion | flops 537657344 | bytes 5242880 | tf_op jit(solution)/shard_map/dot_general | solution.py:117
  21.6 1.2 convolution_convert_fusion.6
  22.9 1.8 divide_multiply_fusion.1
  24.6 58.7 %while.17 = (s32[]{:T(128)}, f32[1,128,128]{2,1,0:T(8,128)S(1)}, f32[1,128]{1,0:T(1,128)S(1)}, f32[16,1,64,128]{3,2,1,0:T(8,128)}, f32[16,1,64,128]{3,2,1,0:T(8,...) while((s32[]{:T(128)}, f32[1,128,128]{2,1,0:T(8,128)S(1)}, ...), condition=%wide.region_3.4_spmd.clone, body=%wide.region_1.3_spmd.clone.sunk | while | flops 8487171 | bytes 5119637 | solution.py:148
  25.4 1.7 fusion.189
  27.3 0.8 fusion.190
  29.1 1.7 fusion.189
  30.9 0.8 fusion.190
  32.8 1.7 fusion.189
  34.6 0.8 fusion.190
  36.4 1.7 fusion.189
  38.3 0.8 fusion.190
  40.1 1.7 fusion.189
  41.9 0.8 fusion.190
  43.8 1.7 fusion.189
  45.6 0.8 fusion.190
  47.4 1.7 fusion.189
  49.3 0.8 fusion.190
  51.1 1.7 fusion.189
  52.9 0.8 fusion.190
  54.8 1.7 fusion.189
  58.4 1.7 fusion.189
  60.3 0.8 fusion.190
  62.1 1.7 fusion.189
  63.9 0.8 fusion.190
  65.8 1.7 fusion.189
  67.6 0.8 fusion.190
  69.4 1.7 fusion.189
  73.1 1.7 fusion.189
  75.0 0.8 fusion.190
  76.8 1.7 fusion.189
  78.6 0.8 fusion.190
  80.4 1.7 fusion.189
  82.3 0.8 fusion.190
  83.4 9.5 %all-gather.2 = bf16[4,129,128]{2,1,0:T(8,128)(2,1)S(1)} all-gather(bf16[1,129,128]{2,1,0:T(8,128)(2,1)S(1)} %maximum_bitcast_fusion), channel_id=2, replica_groups=mesh['sp_0'=8,'sp_1'=4,'tp'=8] {'sp_1'}, dimensions={0}, use_global_device_ids=true | all-gather | bytes 165120 | tf_op jit(solution)/shard_map/all_gather | solution.py:34
  93.1 22.4 %all-gather.3 = bf16[8,129,128]{2,1,0:T(8,128)(2,1)S(1)} all-gather(bf16[1,129,128]{2,1,0:T(8,128)(2,1)S(1)} %maximum_bitcast_fusion.1), channel_id=3, replica_groups=mesh['sp_0'=8,'sp_1'=4,'tp'=8] {'sp_0'}, dimensions={0}, use_global_device_ids=true | all-gather | bytes 297216 | tf_op jit(solution)/shard_map/all_gather | solution.py:34
  115.6 1.7 multiply_reduce_fusion.1
  117.4 3.6 %fusion.48 = bf16[1024,128]{1,0:T(8,128)(2,1)S(1)} fusion(bf16[1024,2048]{1,0:T(8,128)(2,1)} %copy-done.1, bf16[2048,128]{1,0:T(8,128)(2,1)S(1)} %copy-done.16, f32[1024,1,128]{2,0,1:T(8,128)S(1)} %get-tuple-element.181, f32[128]{0:T(128)S(1)} %copy-done.18, f32[1024]{0:T(1024)S(1)} %add_rsqrt_fusion.1), kind=kOutput, calls=%fused_computation.81 | convolution fusion | flops 538181632 | bytes 5509632 | tf_op jit(solution)/shard_map/dot_general | solution.py:117
  121.2 1.3 multiply_reduce_fusion
  122.8 0.9 pad_maximum_fusion.1
  124.3 34.8 %all_to_all.19 = bf16[256,8,256]{0,2,1:T(8,128)(2,1)S(1)} all-to-all(bf16[256,8,256]{0,2,1:T(8,128)(2,1)S(1)} %bitcast.205), channel_id=1, replica_groups=mesh['sp_0'=8,'sp_1'=4,'tp'=8] {'tp'}, dimensions={1} | all-to-all | bytes 2097152 | tf_op jit(solution)/shard_map/all_to_all | solution.py:175
  159.6 16.3 %all-gather.6.cloned.1.call-done = bf16[1024,2048]{1,0:T(8,128)(2,1)} async-done(((bf16[1024,256]{1,0:T(8,128)(2,1)}), bf16[1024,2048]{1,0:T(8,128)(2,1)}) %all-gather.6.cloned.1.call-update) | async-done | bytes 4194320 | tf_op jit(solution)/shard_map/all_gather | solution.py:177
  176.0 4.2 %convolution_convert_fusion = bf16[1024,256]{1,0:T(8,128)(2,1)} fusion(bf16[1024,2048]{1,0:T(8,128)(2,1)} %all-gather.6.cloned.1.call-done, bf16[2048,256]{1,0:T(8,128)(2,1)S(1)} %bitcast.209), kind=kOutput, calls=%fused_computation.48 | convolution fusion | flops 1074003968 | bytes 5767168 | tf_op jit(solution)/shard_map/dot_general | solution.py:176
  (245 shorter events, 21.6 us)
Async XLA Ops:
  6.5 16.3 %copy-start = (bf16[2048,128]{1,0:T(8,128)(2,1)S(1)}, bf16[2048,128]{1,0:T(8,128)(2,1)}, u32[]{:S(2)}) copy-start(bf16[2048,128]{1,0:T(8,128)(2,1)} %param.21) | copy-start | bytes 1572868
  6.5 3.2 %copy-start.9 = (f32[2048]{0:T(1024)S(1)}, f32[2048]{0:T(1024)}, u32[]{:S(2)}) copy-start(f32[2048]{0:T(1024)} %param.19) | copy-start | bytes 24580
  6.5 169.4 %all-gather.6.cloned.1.call-start = ((), (), s32[]{:S(2)}) async-start(), calls=%async_computation.1 | async-start | bytes 4718592 | tf_op jit(solution)/shard_map/all_gather | solution.py:177
  6.5 3.5 %copy-start.4 = (bf16[1024,2048]{1,0:T(8,128)(2,1)S(1)}, bf16[1024,2048]{1,0:T(8,128)(2,1)}, u32[]{:S(2)}) copy-start(bf16[1024,2048]{1,0:T(8,128)(2,1)} %param.18) | copy-start | bytes 12582916
  10.1 1.0 copy-start.5
  11.1 2.7 %copy-start.1 = (bf16[1024,2048]{1,0:T(8,128)(2,1)}, bf16[1024,2048]{1,0:T(8,128)(2,1)S(1)}, u32[]{:S(2)}) copy-start(bf16[1024,2048]{1,0:T(8,128)(2,1)S(1)} %fusion.32) | copy-start | bytes 12582916
  11.1 1.4 copy-start.6
  12.5 5.4 %copy-start.11 = (f32[128]{0:T(128)S(1)}, f32[128]{0:T(128)}, u32[]{:S(2)}) copy-start(f32[128]{0:T(128)} %param.27) | copy-start | bytes 1540
  12.5 5.4 %copy-start.13 = (bf16[2048,128]{1,0:T(8,128)(2,1)S(1)}, bf16[2048,128]{1,0:T(8,128)(2,1)}, u32[]{:S(2)}) copy-start(bf16[2048,128]{1,0:T(8,128)(2,1)} %param.20) | copy-start | bytes 1572868
  13.8 107.2 %collective-permute-start = (bf16[2,128]{1,0:T(2,128)(2,1)S(1)}, bf16[2,128]{1,0:T(2,128)(2,1)S(1)}, u32[]{:S(2)}, u32[]{:S(2)}) collective-permute-start(bf16[2,128]{1,0:T(2,128)(2,1)S(1)} %slice.193), channel_id=1, source_target_pairs={{0,8},{8,16},{16,24},{24,32},{32,40},{40,48},{48,56},{56,64},{64,7... | collective-permute-start | bytes 1544 | tf_op jit(solution)/shard_map/ppermute | solution.py:17
  17.9 3.6 %copy-start.2 = (bf16[1024,2048]{1,0:T(8,128)(2,1)S(1)}, bf16[1024,2048]{1,0:T(8,128)(2,1)}, u32[]{:S(2)}) copy-start(bf16[1024,2048]{1,0:T(8,128)(2,1)} %copy-done.1) | copy-start | bytes 12582916
  18.0 3.6 %copy-start.14 = (bf16[2048,128]{1,0:T(8,128)(2,1)S(1)}, bf16[2048,128]{1,0:T(8,128)(2,1)}, u32[]{:S(2)}) copy-start(bf16[2048,128]{1,0:T(8,128)(2,1)} %param.22) | copy-start | bytes 1572868
  21.6 1.3 copy-start.15
  83.3 34.0 %copy-start.10 = (bf16[3,128]{1,0:T(4,128)(2,1)S(1)}, bf16[3,128]{1,0:T(4,128)(2,1)}, u32[]{:S(2)}) copy-start(bf16[3,128]{1,0:T(4,128)(2,1)} %param.30) | copy-start | bytes 2308
  83.4 34.1 %copy-start.16 = (bf16[2048,128]{1,0:T(8,128)(2,1)S(1)}, bf16[2048,128]{1,0:T(8,128)(2,1)}, u32[]{:S(2)}) copy-start(bf16[2048,128]{1,0:T(8,128)(2,1)} %param.23) | copy-start | bytes 1572868
  83.4 34.1 %copy-start.18 = (f32[128]{0:T(128)S(1)}, f32[128]{0:T(128)}, u32[]{:S(2)}) copy-start(f32[128]{0:T(128)} %param.29) | copy-start | bytes 1540
  117.4 3.7 %copy-start.3 = (bf16[1024,2048]{1,0:T(8,128)(2,1)S(1)}, bf16[1024,2048]{1,0:T(8,128)(2,1)}, u32[]{:S(2)}) copy-start(bf16[1024,2048]{1,0:T(8,128)(2,1)} %copy-done.1) | copy-start | bytes 12582916
  117.4 3.7 %copy-start.17 = (bf16[2048,128]{1,0:T(8,128)(2,1)S(1)}, bf16[2048,128]{1,0:T(8,128)(2,1)}, u32[]{:S(2)}) copy-start(bf16[2048,128]{1,0:T(8,128)(2,1)} %param.25) | copy-start | bytes 1572868
  121.2 1.4 copy-start.12
  121.2 2.5 %copy-start.7 = (bf16[128,2048]{1,0:T(8,128)(2,1)S(1)}, bf16[128,2048]{1,0:T(8,128)(2,1)}, u32[]{:S(2)}) copy-start(bf16[128,2048]{1,0:T(8,128)(2,1)} %param.32) | copy-start | bytes 1572868
  121.2 2.7 %copy-start.8 = (bf16[128,2048]{1,0:T(8,128)(2,1)S(1)}, bf16[128,2048]{1,0:T(8,128)(2,1)}, u32[]{:S(2)}) copy-start(bf16[128,2048]{1,0:T(8,128)(2,1)} %param.33) | copy-start | bytes 1572868
Sparse Core Ops, SparseCore 0:
  123.8 52.1 all-gather.5
where the time goes:
time: 187 us
  blocking collectives  66.6 us (36%)
  other arithmetic  44.8 us (24%)
  matrix products  38.1 us (20%)
  waiting for transfers between devices  16.4 us (9%)
  between operations  13.9 us (7%)
  starting transfers between devices  4.02 us (2%)
  local copies, waits for them, and re-layouts  2.2 us (1%)
    all_to_all x1, blocking collectives, body(): lax.all_to_all(weight_rows, 'tp', split_axis=1, concat_axis=0, tiled=True)  34.8 us
    all_gather x2, blocking collectives, collected_together(): both, at, found = (lax.all_gather(jnp.concatenate(lines), axis), 0, {})  31.9 us
    dot_general x16, other arithmetic, state_block(): scores = jnp.einsum('hid,hjd,hijd->hij', query_blk, key_blk, decay_all)  27.3 us
    all_gather x1, waiting for transfers between devices, body(): lax.all_gather(mixed_here, 'tp', axis=1, tiled=True)  16.3 us
    dot_general x7, matrix products, project(): jnp.dot(normed, weight, preferred_element_type=jnp.float32)  14 us
    dot_general x16, matrix products, state_block(): result = carried + jnp.einsum('hij,hje->hie', scores, value_blk)  12.7 us
    exp x16, other arithmetic, state_block(): decay_all = jnp.exp(jnp.where(causal, diff_log, -jnp.inf))  9.79 us
    dot_general x1, matrix products, body(): jnp.dot(lax.all_gather(mixed_here, 'tp', axis=1, tiled=True), columns, pr...  4.23 us
  transfers between devices with their start and end apart: 2, of which 1 were waited for; matrix products, arithmetic and copies ran while one was open for 38% of the time, Pallas kernels for 0%

commit v1 on v0

--- a/solution.py
+++ b/solution.py
@@ -174,7 +174,9 @@
     weight_rows = jnp.concatenate([out_state, out_conv], axis=0)
     columns = lax.all_to_all(weight_rows, "tp", split_axis=1, concat_axis=0, tiled=True)
     summed = jnp.dot(
-        lax.all_gather(mixed_here, "tp", axis=1, tiled=True),
+        jnp.concatenate(
+            lax.all_to_all(jnp.stack([mixed_here] * lax.axis_size("tp")), "tp", 0, 0), axis=1
+        ),
         columns,
         preferred_element_type=jnp.float32,
     )

time: 187 us -> 228 us (1.22); the launches traced: 187 us -> 225 us
  blocking collectives: 66.6 us -> 94.3 us
  matrix products: 38.1 us -> 60.7 us
  waiting for transfers between devices: 16.4 us -> 0.01 us
  between operations: 13.9 us -> 0.41 us
  local copies, waits for them, and re-layouts: 2.2 us -> 15.3 us
  starting transfers between devices: 4.02 us -> 9.27 us
    all_to_all x1, blocking collectives: 34.8 us -> 62.6 us  [body(): lax.all_to_all(jnp.stack([mixed_here] * lax.axis_size('tp')), 'tp', 0, 0)]
    all_gather x1 -> x0, waiting for transfers between devices: 16.3 us -> none  [body(): lax.all_gather(mixed_here, 'tp', axis=1, tiled=True)]
    squeeze x16, local copies, waits for them, and re-layouts: 0.14 us -> 12.2 us  [body(): lax.scan(state_block, (start_state, start_log), (to_blocks(query_act), to...]
    dot_general x16, matrix products: 3.26 us -> 14.8 us  [state_block(): jnp.einsum('hcd,hce->hde', key_blk * jnp.exp(last_log[:, None, :] - cum_l...]
    dot_general x16, matrix products: 12.7 us -> 24.2 us  [state_block(): result = carried + jnp.einsum('hij,hje->hie', scores, value_blk)]
    all_to_all x0 -> x1, starting transfers between devices: none -> 5.25 us  [body(): lax.all_to_all(weight_rows, 'tp', split_axis=1, concat_axis=0, tiled=True)]
  transfers between devices with their start and end apart: 2 -> 2, of which waited for: 1 -> 0; matrix products, arithmetic and copies ran while one was open for 38% -> 49% of each run, Pallas kernels for 0% -> 0%
where the time goes in v1:
time: 228 us; the launch traced here: 225 us
  blocking collectives  94.3 us (41%)
  matrix products  60.7 us (27%)
  other arithmetic  44.1 us (19%)
  local copies, waits for them, and re-layouts  15.3 us (7%)
  starting transfers between devices  9.27 us (4%)
    all_to_all x1, blocking collectives, body(): lax.all_to_all(jnp.stack([mixed_here] * lax.axis_size('tp')), 'tp', 0, 0)  62.6 us
    all_gather x2, blocking collectives, collected_together(): both, at, found = (lax.all_gather(jnp.concatenate(lines), axis), 0, {})  31.7 us
    dot_general x16, other arithmetic, state_block(): scores = jnp.einsum('hid,hjd,hijd->hij', query_blk, key_blk, decay_all)  27.4 us
    dot_general x16, matrix products, state_block(): result = carried + jnp.einsum('hij,hje->hie', scores, value_blk)  24.2 us
    dot_general x7, matrix products, project(): jnp.dot(normed, weight, preferred_element_type=jnp.float32)  15.8 us
    dot_general x16, matrix products, state_block(): jnp.einsum('hcd,hce->hde', key_blk * jnp.exp(last_log[:, None, :] - cum_l...  14.8 us
    squeeze x16, local copies, waits for them, and re-layouts, body(): lax.scan(state_block, (start_state, start_log), (to_blocks(query_act), to...  12.2 us
    exp x16, other arithmetic, state_block(): decay_all = jnp.exp(jnp.where(causal, diff_log, -jnp.inf))  9.79 us
  transfers between devices with their start and end apart: 2, of which 0 were waited for; matrix products, arithmetic and copies ran while one was open for 49% of the time, Pallas kernels for 0%

profile of v1, /device:TPU:1, one launch (start us, length us, event | category | flops | bytes accessed | tf_op | source)
XLA Modules:
  0.0 224.9 jit_solution(2378140934067303725)
XLA Ops:
  0.0 3.2 %fusion.30 = f32[1024]{0:T(1024)S(1)} fusion(bf16[1024,2048]{1,0:T(8,128)(2,1)} %param.18), kind=kLoop, calls=%fused_computation.44 | loop fusion | flops 6290432 | bytes 4198400 | tf_op jit(solution)/shard_map/reduce_sum | solution.py:66
  6.0 1.3 fusion.44
  7.3 4.0 %collective-permute-start = (bf16[2,128]{1,0:T(2,128)(2,1)S(1)}, bf16[2,128]{1,0:T(2,128)(2,1)S(1)}, u32[]{:S(2)}, u32[]{:S(2)}) collective-permute-start(bf16[2,128]{1,0:T(2,128)(2,1)S(1)} %slice.193), channel_id=1, source_target_pairs={{0,8},{8,16},{16,24},{24,32},{32,40},{40,48},{48,56},{56,64},{64,7... | collective-permute-start | bytes 1544 | tf_op jit(solution)/shard_map/ppermute | solution.py:17
  12.0 1.3 copy.57
  13.3 5.2 %all-to-all-start.1 = ((bf16[256,8,256]{2,0,1:T(8,128)(2,1)}), bf16[256,8,256]{2,0,1:T(8,128)(2,1)S(1)}, u32[]{:S(2)}, u32[]{:S(2)}) async-start(bf16[256,8,256]{2,0,1:T(8,128)(2,1)} %copy.57), calls=%async_computation.1 | async-start | bytes 2097152 | tf_op jit(solution)/shard_map/all_to_all | solution.py:175
  18.6 3.7 %divide_multiply_fusion = f32[1024,128]{1,0:T(8,128)S(1)} fusion(bf16[1024,2048]{1,0:T(8,128)(2,1)} %copy-done.1, bf16[2048,128]{1,0:T(8,128)(2,1)} %param.20), kind=kOutput, calls=%fused_computation.87 | convolution fusion | flops 537657344 | bytes 5242880 | tf_op jit(solution)/shard_map/dot_general | solution.py:117
  22.3 2.0 convolution_convert_fusion.5
  24.3 2.6 %divide_multiply_fusion.1 = (f32[1024,128]{1,0:T(8,128)S(1)}, f32[1024,128]{1,0:T(8,128)}) fusion(f32[128]{0:T(128)S(1)} %get-tuple-element.166, f32[1024,128]{1,0:T(8,128)S(1)} %copy-done.14, f32[128]{0:T(128)S(1)} %get-tuple-element.168, f32[128]{0:T(128)S(1)} %get-tuple-element.167, bf16[1024,2048]{1,0:T(8,128)(2,1)S(1)} %copy-done.2, ...), kind=kOutput, calls=%fused_computation.88 | convolution fusion | flops 539885568 | bytes 6292992 | tf_op jit(solution)/shard_map/dot_general | solution.py:117
  26.9 93.7 %while.17 = (s32[]{:T(128)}, f32[1,128,128]{2,1,0:T(8,128)S(1)}, f32[1,128]{1,0:T(1,128)S(1)}, f32[16,1,64,128]{3,2,1,0:T(8,128)}, f32[16,1,64,128]{3,2,1,0:T(8,...) while((s32[]{:T(128)}, f32[1,128,128]{2,1,0:T(8,128)S(1)}, ...), condition=%wide.region_3.4_spmd.clone, body=%wide.region_1.3_spmd.clone.sunk | while | flops 8487171 | bytes 5111445 | solution.py:148
  28.4 1.7 fusion.196
  30.3 1.5 fusion.197
  34.3 1.7 fusion.196
  36.1 1.5 fusion.197
  40.1 1.7 fusion.196
  42.0 1.5 fusion.197
  46.0 1.7 fusion.196
  47.8 1.5 fusion.197
  51.8 1.7 fusion.196
  53.7 1.5 fusion.197
  57.7 1.7 fusion.196
  59.6 1.5 fusion.197
  63.6 1.7 fusion.196
  65.4 1.5 fusion.197
  69.4 1.7 fusion.196
  71.3 1.5 fusion.197
  75.3 1.7 fusion.196
  77.1 1.5 fusion.197
  81.1 1.7 fusion.196
  83.0 1.5 fusion.197
  87.0 1.7 fusion.196
  88.8 1.5 fusion.197
  92.9 1.7 fusion.196
  94.7 1.5 fusion.197
  98.7 1.7 fusion.196
  100.6 1.5 fusion.197
  104.6 1.7 fusion.196
  106.4 1.5 fusion.197
  110.4 1.7 fusion.196
  112.3 1.5 fusion.197
  116.3 1.7 fusion.196
  118.1 1.5 fusion.197
  120.7 9.4 %all-gather.2 = bf16[4,129,128]{2,1,0:T(8,128)(2,1)S(1)} all-gather(bf16[1,129,128]{2,1,0:T(8,128)(2,1)S(1)} %maximum_bitcast_fusion), channel_id=2, replica_groups=mesh['sp_0'=8,'sp_1'=4,'tp'=8] {'sp_1'}, dimensions={0}, use_global_device_ids=true | all-gather | bytes 165120 | tf_op jit(solution)/shard_map/all_gather | solution.py:34
  130.2 22.3 %all-gather.3 = bf16[8,129,128]{2,1,0:T(8,128)(2,1)S(1)} all-gather(bf16[1,129,128]{2,1,0:T(8,128)(2,1)S(1)} %maximum_bitcast_fusion.1), channel_id=3, replica_groups=mesh['sp_0'=8,'sp_1'=4,'tp'=8] {'sp_0'}, dimensions={0}, use_global_device_ids=true | all-gather | bytes 297216 | tf_op jit(solution)/shard_map/all_gather | solution.py:34
  152.7 1.7 multiply_reduce_fusion.1
  154.5 3.7 %fusion.57 = bf16[1024,128]{1,0:T(8,128)(2,1)S(1)} fusion(bf16[1024,2048]{1,0:T(8,128)(2,1)} %copy-done.1, bf16[2048,128]{1,0:T(8,128)(2,1)} %param.23, f32[1024,1,128]{2,0,1:T(8,128)S(1)} %get-tuple-element.172, f32[128]{0:T(128)S(1)} %copy-done.16, f32[1024]{0:T(1024)S(1)} %add_rsqrt_fusion.1), kind=kOutput, calls=%fused_computation.85 | convolution fusion | flops 538181632 | bytes 5509632 | tf_op jit(solution)/shard_map/dot_general | solution.py:117
  158.4 1.3 multiply_reduce_fusion
  160.3 62.6 %all_to_all.21 = bf16[8,1024,256]{2,1,0:T(8,128)(2,1)S(1)} all-to-all(bf16[8,1024,256]{2,1,0:T(8,128)(2,1)S(1)} %stack.2), channel_id=1, replica_groups=mesh['sp_0'=8,'sp_1'=4,'tp'=8] {'tp'}, dimensions={0} | all-to-all | bytes 8388608 | tf_op jit(solution)/shard_map/all_to_all | solution.py:178
  222.9 2.1 fusion.38
  (241 shorter events, 45.6 us)
Async XLA Ops:
  0.0 24.3 %copy-start = (bf16[2048,128]{1,0:T(8,128)(2,1)S(1)}, bf16[2048,128]{1,0:T(8,128)(2,1)}, u32[]{:S(2)}) copy-start(bf16[2048,128]{1,0:T(8,128)(2,1)} %param.21) | copy-start | bytes 1572868
  0.0 3.5 %copy-start.4 = (bf16[1024,2048]{1,0:T(8,128)(2,1)S(1)}, bf16[1024,2048]{1,0:T(8,128)(2,1)}, u32[]{:S(2)}) copy-start(bf16[1024,2048]{1,0:T(8,128)(2,1)} %param.18) | copy-start | bytes 12582916
  0.0 3.5 %copy-start.9 = (f32[2048]{0:T(1024)S(1)}, f32[2048]{0:T(1024)}, u32[]{:S(2)}) copy-start(f32[2048]{0:T(1024)} %param.19) | copy-start | bytes 24580
  3.5 1.0 copy-start.5
  4.6 2.7 %copy-start.1 = (bf16[1024,2048]{1,0:T(8,128)(2,1)}, bf16[1024,2048]{1,0:T(8,128)(2,1)S(1)}, u32[]{:S(2)}) copy-start(bf16[1024,2048]{1,0:T(8,128)(2,1)S(1)} %fusion.32) | copy-start | bytes 12582916
  4.6 1.4 copy-start.6
  6.0 5.3 %copy-start.7 = (bf16[128,2048]{1,0:T(8,128)(2,1)S(1)}, bf16[128,2048]{1,0:T(8,128)(2,1)}, u32[]{:S(2)}) copy-start(bf16[128,2048]{1,0:T(8,128)(2,1)} %param.32) | copy-start | bytes 1572868
  6.0 5.6 %copy-start.8 = (bf16[128,2048]{1,0:T(8,128)(2,1)S(1)}, bf16[128,2048]{1,0:T(8,128)(2,1)}, u32[]{:S(2)}) copy-start(bf16[128,2048]{1,0:T(8,128)(2,1)} %param.33) | copy-start | bytes 1572868
  7.2 11.3 %copy-start.11 = (f32[128]{0:T(128)S(1)}, f32[128]{0:T(128)}, u32[]{:S(2)}) copy-start(f32[128]{0:T(128)} %param.27) | copy-start | bytes 1540
  7.3 151.0 %collective-permute-start = (bf16[2,128]{1,0:T(2,128)(2,1)S(1)}, bf16[2,128]{1,0:T(2,128)(2,1)S(1)}, u32[]{:S(2)}, u32[]{:S(2)}) collective-permute-start(bf16[2,128]{1,0:T(2,128)(2,1)S(1)} %slice.193), channel_id=1, source_target_pairs={{0,8},{8,16},{16,24},{24,32},{32,40},{40,48},{48,56},{56,64},{64,7... | collective-permute-start | bytes 1544 | tf_op jit(solution)/shard_map/ppermute | solution.py:17
  13.3 146.7 %all-to-all-start.1 = ((bf16[256,8,256]{2,0,1:T(8,128)(2,1)}), bf16[256,8,256]{2,0,1:T(8,128)(2,1)S(1)}, u32[]{:S(2)}, u32[]{:S(2)}) async-start(bf16[256,8,256]{2,0,1:T(8,128)(2,1)} %copy.57), calls=%async_computation.1 | async-start | bytes 2097152 | tf_op jit(solution)/shard_map/all_to_all | solution.py:175
  18.6 3.7 %copy-start.2 = (bf16[1024,2048]{1,0:T(8,128)(2,1)S(1)}, bf16[1024,2048]{1,0:T(8,128)(2,1)}, u32[]{:S(2)}) copy-start(bf16[1024,2048]{1,0:T(8,128)(2,1)} %copy-done.1) | copy-start | bytes 12582916
  18.6 3.7 %copy-start.13 = (bf16[2048,128]{1,0:T(8,128)(2,1)S(1)}, bf16[2048,128]{1,0:T(8,128)(2,1)}, u32[]{:S(2)}) copy-start(bf16[2048,128]{1,0:T(8,128)(2,1)} %param.22) | copy-start | bytes 1572868
  22.3 2.0 copy-start.14
  120.6 33.9 %copy-start.10 = (bf16[3,128]{1,0:T(4,128)(2,1)S(1)}, bf16[3,128]{1,0:T(4,128)(2,1)}, u32[]{:S(2)}) copy-start(bf16[3,128]{1,0:T(4,128)(2,1)} %param.30) | copy-start | bytes 2308
  120.6 33.9 %copy-start.16 = (f32[128]{0:T(128)S(1)}, f32[128]{0:T(128)}, u32[]{:S(2)}) copy-start(f32[128]{0:T(128)} %param.29) | copy-start | bytes 1540
  154.5 3.8 %copy-start.3 = (bf16[1024,2048]{1,0:T(8,128)(2,1)S(1)}, bf16[1024,2048]{1,0:T(8,128)(2,1)}, u32[]{:S(2)}) copy-start(bf16[1024,2048]{1,0:T(8,128)(2,1)} %copy-done.1) | copy-start | bytes 12582916
  154.5 3.8 %copy-start.15 = (bf16[2048,128]{1,0:T(8,128)(2,1)S(1)}, bf16[2048,128]{1,0:T(8,128)(2,1)}, u32[]{:S(2)}) copy-start(bf16[2048,128]{1,0:T(8,128)(2,1)} %param.25) | copy-start | bytes 1572868
  158.4 1.4 copy-start.12
